TPU v7x, 32 devices: a whole 2x2x4 slice. The times are simulated.
32 devices in a mesh: fs: 8 (over z, y), tp: 4 (over x, core).
Axes of the slice: x: 2, y: 2, z: 4, core: 2. Of those that a mesh axis runs over, the one named last changes fastest.
Arguments:
- saved_input: bfloat16 [65536, 2048], P(('fs', 'tp')), may hold values from -500 to 500
- value_cotangent: bfloat16 [65536, 1024], P(('fs', 'tp')), may hold values from -500 to 500
- hidden_input: bfloat16 [65536, 1024], P(('fs', 'tp')), may hold values from -500 to 500
- out_cotangent: bfloat16 [65536, 2048], P(('fs', 'tp')), may hold values from -500 to 500
- value_factor: bfloat16 [2048, 256], P('fs'), may hold values from -2 to 2
- out_factor: bfloat16 [1024, 256], P('fs'), may hold values from -2 to 2
- value_weight: float32 [2048, 1024], P('fs', 'tp'), may hold values from -0.125 to 0.125
- out_weight: float32 [1024, 2048], P('fs', 'tp'), may hold values from -0.1875 to 0.1875
- value_first: float32 [256, 1024], P('fs', 'tp'), may hold values from -1.2 to 1.2
- value_second: float32 [256, 1024], P('fs', 'tp'), may hold values from 0.02 to 0.5
- out_first: float32 [256, 2048], P('fs', 'tp'), may hold values from -1.2 to 1.2
- out_second: float32 [256, 2048], P('fs', 'tp'), may hold values from 0.02 to 0.5
Outputs:
- value_update: float32 [2048, 1024], P('fs', 'tp')
- out_update: float32 [1024, 2048], P('fs', 'tp')
- new_value_weight: float32 [2048, 1024], P('fs', 'tp')
- new_out_weight: float32 [1024, 2048], P('fs', 'tp')
- value_copy: bfloat16 [2048, 1024], P(None, 'tp')
- out_copy: bfloat16 [1024, 2048], P(None, 'tp')
- new_value_first: float32 [256, 1024], P('fs', 'tp')
- new_value_second: float32 [256, 1024], P('fs', 'tp')
- new_out_first: float32 [256, 2048], P('fs', 'tp')
- new_out_second: float32 [256, 2048], P('fs', 'tp')
All inputs are finite; a program needn't handle non-finite values.
Results may differ from a plain program's by a relative error of at most 0.0065.
Values may be sent and summed in bfloat16 or wider, within the bound.
A program may use at most 128 MiB of HBM per device.

v0:
```python
import jax
import jax.numpy as jnp
from jax import lax
from jax.sharding import PartitionSpec as P

D = 2048
DM = 1024
R = 256
momentum_decay = 0.9
square_decay = 0.95
adam_epsilon = 1e-08
update_scale = 0.25
learning_rate = 0.01


def moment_ratio(first, second, lowrank, clip_factor):
    scaled = clip_factor * lowrank
    new_first = momentum_decay * first + (1.0 - momentum_decay) * scaled
    new_second = square_decay * second + (1.0 - square_decay) * scaled * scaled
    ratio = new_first / (jnp.sqrt(new_second) + adam_epsilon)
    return (new_first, new_second, ratio)


def input_times_factor(inputs, factor):
    return jnp.dot(
        inputs, lax.all_gather(factor, "fs", axis=0, tiled=True), preferred_element_type=jnp.float32
    )


def split_product(basis, cotangents):
    basis_high = basis.astype(jnp.bfloat16)
    basis_rest = (basis - basis_high.astype(jnp.float32)).astype(jnp.bfloat16)
    high_part = jnp.einsum("tr,tc->rc", basis_high, cotangents, preferred_element_type=jnp.float32)
    rest_part = jnp.einsum("tr,tc->rc", basis_rest, cotangents, preferred_element_type=jnp.float32)
    return high_part + rest_part


def shards(
    saved_input,
    value_cotangent,
    hidden_input,
    out_cotangent,
    value_factor,
    out_factor,
    value_weight,
    out_weight,
    value_first,
    value_second,
    out_first,
    out_second,
):
    highest = lax.Precision.HIGHEST
    value_basis = input_times_factor(saved_input, value_factor)
    out_basis = input_times_factor(hidden_input, out_factor)
    left = value_basis
    right = out_basis
    first_part = split_product(left, value_cotangent)
    second_part = split_product(right, out_cotangent)
    lowrank = lax.psum_scatter(
        jnp.concatenate([first_part, second_part], axis=1), "fs", scatter_dimension=0, tiled=True
    )
    low_value, low_out = (
        lax.psum_scatter(lowrank[:, :DM], "tp", scatter_dimension=1, tiled=True),
        lax.psum_scatter(lowrank[:, DM:], "tp", scatter_dimension=1, tiled=True),
    )
    squares = lax.psum((jnp.sum(low_value * low_value), jnp.sum(low_out * low_out)), ("fs", "tp"))
    root_mean = jnp.sqrt((squares[0] + squares[1]) / (R * (D + DM)))
    clip_factor = 1.0 / jnp.maximum(root_mean, 1.0)
    new_value_first, new_value_second, value_ratio = moment_ratio(
        value_first, value_second, low_value, clip_factor
    )
    new_out_first, new_out_second, out_ratio = moment_ratio(
        out_first, out_second, low_out, clip_factor
    )
    left = value_factor.astype(jnp.float32)
    right = out_factor.astype(jnp.float32)
    value_sum = jnp.dot(
        left, lax.all_gather(value_ratio, "fs", axis=0, tiled=True), precision=highest
    )
    out_sum = jnp.dot(right, lax.all_gather(out_ratio, "fs", axis=0, tiled=True), precision=highest)
    value_update = update_scale * value_sum
    out_update = update_scale * out_sum
    new_value_weight = value_weight - learning_rate * value_update
    new_out_weight = out_weight - learning_rate * out_update
    value_copy, out_copy = (
        lax.all_gather(new_value_weight.astype(jnp.bfloat16), "fs", axis=0, tiled=True),
        lax.all_gather(new_out_weight.astype(jnp.bfloat16), "fs", axis=0, tiled=True),
    )
    return (
        value_update,
        out_update,
        new_value_weight,
        new_out_weight,
        value_copy,
        out_copy,
        new_value_first,
        new_value_second,
        new_out_first,
        new_out_second,
    )


def solution(mesh):
    placed = (
        P(("fs", "tp"), None),
        P(("fs", "tp"), None),
        P(("fs", "tp"), None),
        P(("fs", "tp"), None),
        P("fs", None),
        P("fs", None),
        P("fs", "tp"),
        P("fs", "tp"),
        P("fs", "tp"),
        P("fs", "tp"),
        P("fs", "tp"),
        P("fs", "tp"),
    )
    return jax.shard_map(
        shards,
        mesh=mesh,
        in_specs=placed,
        out_specs=(
            P("fs", "tp"),
            P("fs", "tp"),
            P("fs", "tp"),
            P("fs", "tp"),
            P(None, "tp"),
            P(None, "tp"),
            P("fs", "tp"),
            P("fs", "tp"),
            P("fs", "tp"),
            P("fs", "tp"),
        ),
        check_vma=False,
    )
```

profile of v0, /device:TPU:0, one launch (start us, length us, event | category | flops | bytes accessed | tf_op | source)
XLA Modules:
  0.0 351.5 jit_solution(5440025133149684813)
XLA Ops:
  8.0 33.6 %all_gather.19 = bf16[1024,256]{1,0:T(8,128)(2,1)S(1)} all-gather(bf16[128,256]{1,0:T(8,128)(2,1)} %param.17), channel_id=1, replica_groups=mesh['fs'=8,'tp'=4] {'fs'}, dimensions={0}, use_global_device_ids=true | all-gather | bytes 589824 | tf_op jit(solution)/shard_map/all_gather | solution.py:26
  41.6 3.4 fusion.13
  45.1 2.3 fusion.1
  47.4 2.4 convolution_add_fusion
  49.8 4.3 %all-gather.4.cloned.1.call-done = bf16[2048,256]{1,0:T(8,128)(2,1)} async-done(((bf16[256,256]{1,0:T(8,128)(2,1)}), bf16[2048,256]{1,0:T(8,128)(2,1)}) %all-gather.4.cloned.1.call-update) | async-done | bytes 1048592 | tf_op jit(solution)/shard_map/all_gather | solution.py:26
  54.1 6.2 %fusion.12 = f32[2048,256]{1,0:T(8,128)S(1)} fusion(bf16[2048,2048]{1,0:T(8,128)(2,1)} %param.12, bf16[2048,256]{1,0:T(8,128)(2,1)} %all-gather.4.cloned.1.call-done), kind=kOutput, calls=%fused_computation.27 | convolution fusion | flops 2147483648 | bytes 11534336 | tf_op jit(solution)/shard_map/dot_general | solution.py:25
  60.3 1.3 fusion.4
  62.9 1.9 pad_maximum_fusion
  64.9 73.3 %reduce-scatter.4.cloned.1.call-done = f32[32,3072]{1,0:T(8,128)} async-done(((f32[256,3072]{1,0:T(8,128)}), f32[32,3072]{1,0:T(8,128)}) %reduce-scatter.4.cloned.1.call-update) | async-done | bytes 393232 | tf_op jit(solution)/shard_map/reduce_scatter | solution.py:59
  138.3 1.6 slice.8
  139.9 1.7 slice.9
  141.7 18.4 %reduce-scatter.6.cloned.1.call-done = f32[32,256]{1,0:T(8,128)} async-done(((f32[32,1024]{1,0:T(8,128)}), f32[32,256]{1,0:T(8,128)}) %reduce-scatter.6.cloned.1.call-update) | async-done | bytes 32784 | tf_op jit(solution)/shard_map/reduce_scatter | solution.py:63
  160.1 1.4 multiply_reduce_fusion.1
  161.5 21.6 %reduce-scatter.8.cloned.1.call-done = f32[32,512]{1,0:T(8,128)} async-done(((f32[32,2048]{1,0:T(8,128)}), f32[32,512]{1,0:T(8,128)}) %reduce-scatter.8.cloned.1.call-update) | async-done | bytes 65552 | tf_op jit(solution)/shard_map/reduce_scatter | solution.py:64
  183.1 1.5 multiply_reduce_fusion
  186.0 39.3 %psum.16 = f32[]{:T(128)} all-reduce(f32[]{:T(128)S(6)} %add.45), channel_id=1, replica_groups=mesh['fs'=8,'tp'=4] {'fs','tp'}, use_global_device_ids=true, to_apply=%region_3.0 | all-reduce | flops 1 | bytes 8 | tf_op jit(solution)/shard_map/psum | solution.py:66
  226.0 1.5 add_divide_fusion
  227.6 31.2 %all_gather.21 = f32[256,512]{1,0:T(8,128)S(1)} all-gather(f32[32,512]{1,0:T(8,128)S(1)} %get-tuple-element.24), channel_id=1, replica_groups=mesh['fs'=8,'tp'=4] {'fs'}, dimensions={0}, use_global_device_ids=true | all-gather | bytes 589824 | tf_op jit(solution)/shard_map/all_gather | solution.py:80
  258.8 1.3 fusion.8
  261.0 31.0 %all_gather.20 = f32[256,256]{1,0:T(8,128)S(1)} all-gather(f32[32,256]{1,0:T(8,128)S(1)} %get-tuple-element.27), channel_id=1, replica_groups=mesh['fs'=8,'tp'=4] {'fs'}, dimensions={0}, use_global_device_ids=true | all-gather | bytes 294912 | tf_op jit(solution)/shard_map/all_gather | solution.py:78
  296.4 5.1 %all-gather.8.cloned.1.call-done = bf16[1024,512]{0,1:T(8,128)(2,1)} async-done(((bf16[128,512]{0,1:T(8,128)(2,1)}), bf16[1024,512]{0,1:T(8,128)(2,1)}) %all-gather.8.cloned.1.call-update) | async-done | bytes 1048592 | tf_op jit(solution)/shard_map/all_gather | solution.py:87
  301.5 2.3 copy.29
  303.8 38.6 %all-gather.6.cloned.1.call-done = bf16[2048,256]{0,1:T(8,128)(2,1)} async-done(((bf16[256,256]{0,1:T(8,128)(2,1)}), bf16[2048,256]{0,1:T(8,128)(2,1)}) %all-gather.6.cloned.1.call-update) | async-done | bytes 1048592 | tf_op jit(solution)/shard_map/all_gather | solution.py:86
  342.4 2.3 copy.28
  (45 shorter events, 7.7 us)
Async XLA Ops:
  7.2 46.9 %all-gather.4.cloned.1.call-start = ((), (), s32[]{:S(2)}) async-start(), calls=%async_computation.3 | async-start | bytes 1179648 | tf_op jit(solution)/shard_map/all_gather | solution.py:26
  7.9 130.4 %reduce-scatter.4.cloned.1.call-start = ((), (), s32[]{:S(2)}) async-start(), calls=%async_computation.4 | async-start | bytes 3538944 | tf_op jit(solution)/shard_map/reduce_scatter | solution.py:59
  8.0 37.1 %copy-start = (bf16[2048,2048]{1,0:T(8,128)(2,1)S(1)}, bf16[2048,2048]{1,0:T(8,128)(2,1)}, u32[]{:S(2)}) copy-start(bf16[2048,2048]{1,0:T(8,128)(2,1)} %param.15) | copy-start | bytes 25165828
  54.1 6.3 %copy-start.10 = (bf16[2048,1024]{1,0:T(8,128)(2,1)S(1)}, bf16[2048,1024]{1,0:T(8,128)(2,1)}, u32[]{:S(2)}) copy-start(bf16[2048,1024]{1,0:T(8,128)(2,1)} %param.13) | copy-start | bytes 12582916
  64.8 121.0 %copy-start.3 = (f32[128,512]{1,0:T(8,128)S(1)}, f32[128,512]{1,0:T(8,128)}, u32[]{:S(2)}) copy-start(f32[128,512]{1,0:T(8,128)} %param.19) | copy-start | bytes 786436
  64.8 161.2 %copy-start.6 = (f32[32,512]{1,0:T(8,128)S(1)}, f32[32,512]{1,0:T(8,128)}, u32[]{:S(2)}) copy-start(f32[32,512]{1,0:T(8,128)} %param.23) | copy-start | bytes 196612
  64.8 161.2 %copy-start.7 = (f32[32,512]{1,0:T(8,128)S(1)}, f32[32,512]{1,0:T(8,128)}, u32[]{:S(2)}) copy-start(f32[32,512]{1,0:T(8,128)} %param.22) | copy-start | bytes 196612
  64.8 194.0 %copy-start.2 = (bf16[128,256]{1,0:T(8,128)(2,1)S(1)}, bf16[128,256]{1,0:T(8,128)(2,1)}, u32[]{:S(2)}) copy-start(bf16[128,256]{1,0:T(8,128)(2,1)} %param.17) | copy-start | bytes 196612
  64.8 195.3 %copy-start.4 = (f32[256,256]{1,0:T(8,128)S(1)}, f32[256,256]{1,0:T(8,128)}, u32[]{:S(2)}) copy-start(f32[256,256]{1,0:T(8,128)} %param.18) | copy-start | bytes 786436
  64.8 195.4 %copy-start.8 = (f32[32,256]{1,0:T(8,128)S(1)}, f32[32,256]{1,0:T(8,128)}, u32[]{:S(2)}) copy-start(f32[32,256]{1,0:T(8,128)} %param.21) | copy-start | bytes 98308
  64.9 195.4 %copy-start.9 = (f32[32,256]{1,0:T(8,128)S(1)}, f32[32,256]{1,0:T(8,128)}, u32[]{:S(2)}) copy-start(f32[32,256]{1,0:T(8,128)} %param.20) | copy-start | bytes 98308
  64.9 227.1 %copy-start.1 = (bf16[256,256]{1,0:T(8,128)(2,1)S(1)}, bf16[256,256]{1,0:T(8,128)(2,1)}, u32[]{:S(2)}) copy-start(bf16[256,256]{1,0:T(8,128)(2,1)} %param.16) | copy-start | bytes 393220
  64.9 95.2 %reduce-scatter.6.cloned.1.call-start = ((), (), s32[]{:S(2)}) async-start(), calls=%async_computation.5 | async-start | bytes 163840 | tf_op jit(solution)/shard_map/reduce_scatter | solution.py:63
  139.9 43.2 %reduce-scatter.8.cloned.1.call-start = ((), (), s32[]{:S(2)}) async-start(), calls=%async_computation.6 | async-start | bytes 327680 | tf_op jit(solution)/shard_map/reduce_scatter | solution.py:64
  141.6 159.9 %all-gather.8.cloned.1.call-start = ((), (), s32[]{:S(2)}) async-start(), calls=%async_computation.8 | async-start | bytes 1179648 | tf_op jit(solution)/shard_map/all_gather | solution.py:87
  160.1 100.2 %copy-start.5 = (f32[32,256]{1,0:T(8,128)S(1)}, f32[32,256]{1,0:T(8,128)}, u32[]{:S(2)}) copy-start(f32[32,256]{1,0:T(8,128)} %reduce-scatter.6.cloned.1.call-done) | copy-start | bytes 98308
  260.1 82.4 %all-gather.6.cloned.1.call-start = ((), (), s32[]{:S(2)}) async-start(), calls=%async_computation.7 | async-start | bytes 1179648 | tf_op jit(solution)/shard_map/all_gather | solution.py:86
Sparse Core Ops, SparseCore 0:
  10.1 43.9 all-gather.3
  65.0 73.2 reduce-scatter.3
  141.3 18.7 reduce-scatter.5
  162.9 20.0 reduce-scatter.7
  260.2 41.2 all-gather.7
  304.0 38.3 all-gather.5
where the time goes:
time: 352 us
  waiting for transfers between devices  162 us (46%)
  blocking collectives  135 us (38%)
  matrix products  19.3 us (5%)
  between operations  16.3 us (5%)
  local copies, waits for them, and re-layouts  11.4 us (3%)
  other arithmetic  7.01 us (2%)
    reduce_scatter x1, waiting for transfers between devices, shards(): lax.psum_scatter(jnp.concatenate([first_part, second_part], axis=1), 'fs'...  73.3 us
    psum x1, blocking collectives, shards(): lax.psum((jnp.sum(low_value * low_value), jnp.sum(low_out * low_out)), ('...  39.3 us
    all_gather x1, waiting for transfers between devices, shards(): lax.all_gather(new_value_weight.astype(jnp.bfloat16), 'fs', axis=0, tiled...  38.6 us
    all_gather x1, blocking collectives, input_times_factor(): lax.all_gather(factor, 'fs', axis=0, tiled=True)  33.6 us
    all_gather x1, blocking collectives, shards(): lax.all_gather(out_ratio, 'fs', axis=0, tiled=True)  31.2 us
    all_gather x1, blocking collectives, shards(): lax.all_gather(value_ratio, 'fs', axis=0, tiled=True)  31 us
    reduce_scatter x1, waiting for transfers between devices, shards(): lax.psum_scatter(lowrank[:, DM:], 'tp', scatter_dimension=1, tiled=True)  21.6 us
    reduce_scatter x1, waiting for transfers between devices, shards(): lax.psum_scatter(lowrank[:, :DM], 'tp', scatter_dimension=1, tiled=True)  18.4 us
  transfers between devices with their start and end apart: 6, of which 6 were waited for; matrix products, arithmetic and copies ran while one was open for 5% of the time, Pallas kernels for 0%

commit v1 on v0

--- a/solution.py
+++ b/solution.py
@@ -1,3 +1,4 @@
+import functools
 import jax
 import jax.numpy as jnp
 from jax import lax
@@ -11,6 +12,24 @@
 adam_epsilon = 1e-08
 update_scale = 0.25
 learning_rate = 0.01
+
+
+def _pass_copies(in_array, shard_axis):
+    carry_in = lax.psum(1, shard_axis)
+    aux, f_next = (carry_in, lax.axis_index(shard_axis))
+    m_next, raw_out = (in_array, 1)
+    while raw_out < aux:
+        arr_next = map(lambda p: (p, p ^ raw_out), range(aux))
+        current_value = list(arr_next)
+        z1 = lax.ppermute(m_next, shard_axis, current_value)
+        top = jnp.concatenate([m_next, z1], axis=0)
+        even = jnp.concatenate([z1, m_next], axis=0)
+        m_next = jnp.where(f_next & raw_out == 0, top, even)
+        raw_out = 2 * raw_out
+    return m_next
+
+
+_register_spans = functools.partial(_pass_copies, shard_axis="fs")
 
 
 def moment_ratio(first, second, lowrank, clip_factor):
@@ -74,9 +93,7 @@
     )
     left = value_factor.astype(jnp.float32)
     right = out_factor.astype(jnp.float32)
-    value_sum = jnp.dot(
-        left, lax.all_gather(value_ratio, "fs", axis=0, tiled=True), precision=highest
-    )
+    value_sum = jnp.dot(left, _register_spans(value_ratio), precision=highest)
     out_sum = jnp.dot(right, lax.all_gather(out_ratio, "fs", axis=0, tiled=True), precision=highest)
     value_update = update_scale * value_sum
     out_update = update_scale * out_sum

time: 352 us -> 352 us (level)
  blocking collectives: 135 us -> 104 us
  waiting for transfers between devices: 162 us -> 190 us
    all_gather x1 -> x0, blocking collectives: 31 us -> none  [shards(): lax.all_gather(value_ratio, 'fs', axis=0, tiled=True)]
    all_gather x1, waiting for transfers between devices: 5.13 us -> 19.3 us  [shards(): lax.all_gather(new_out_weight.astype(jnp.bfloat16), 'fs', axis=0, tiled=T...]
    ppermute x0 -> x3, waiting for transfers between devices: none -> 13.2 us  [_pass_copies(): z1 = lax.ppermute(m_next, shard_axis, current_value)]
  transfers between devices with their start and end apart: 6 -> 9, of which waited for: 6 -> 9; matrix products, arithmetic and copies ran while one was open for 5% -> 5% of each run, Pallas kernels for 0% -> 0%
where the time goes in v1:
time: 352 us; the launch traced here: 351 us
  waiting for transfers between devices  190 us (54%)
  blocking collectives  104 us (30%)
  matrix products  19.3 us (5%)
  between operations  16.4 us (5%)
  local copies, waits for them, and re-layouts  11.4 us (3%)
  other arithmetic  7.03 us (2%)
    reduce_scatter x1, waiting for transfers between devices, shards(): lax.psum_scatter(jnp.concatenate([first_part, second_part], axis=1), 'fs'...  73.4 us
    psum x1, blocking collectives, shards(): lax.psum((jnp.sum(low_value * low_value), jnp.sum(low_out * low_out)), ('...  39.3 us
    all_gather x1, waiting for transfers between devices, shards(): lax.all_gather(new_value_weight.astype(jnp.bfloat16), 'fs', axis=0, tiled...  38.6 us
    all_gather x1, blocking collectives, input_times_factor(): lax.all_gather(factor, 'fs', axis=0, tiled=True)  33.6 us
    all_gather x1, blocking collectives, shards(): lax.all_gather(out_ratio, 'fs', axis=0, tiled=True)  31.2 us
    reduce_scatter x1, waiting for transfers between devices, shards(): lax.psum_scatter(lowrank[:, DM:], 'tp', scatter_dimension=1, tiled=True)  21.6 us
    all_gather x1, waiting for transfers between devices, shards(): lax.all_gather(new_out_weight.astype(jnp.bfloat16), 'fs', axis=0, tiled=T...  19.3 us
    reduce_scatter x1, waiting for transfers between devices, shards(): lax.psum_scatter(lowrank[:, :DM], 'tp', scatter_dimension=1, tiled=True)  18.4 us
  transfers between devices with their start and end apart: 9, of which 9 were waited for; matrix products, arithmetic and copies ran while one was open for 5% of the time, Pallas kernels for 0%

profile of v1, /device:TPU:0, one launch (start us, length us, event | category | flops | bytes accessed | tf_op | source)
XLA Modules:
  0.0 351.2 jit_solution(12720617944059998353)
XLA Ops:
  8.0 33.6 %all_gather.16 = bf16[1024,256]{1,0:T(8,128)(2,1)S(1)} all-gather(bf16[128,256]{1,0:T(8,128)(2,1)} %param.17), channel_id=1, replica_groups=mesh['fs'=8,'tp'=4] {'fs'}, dimensions={0}, use_global_device_ids=true | all-gather | bytes 589824 | tf_op jit(solution)/shard_map/all_gather | solution.py:45
  41.6 3.4 fusion.21
  45.1 2.3 fusion.1
  47.4 2.4 convolution_add_fusion
  49.8 4.3 %all-gather.4.cloned.1.call-done = bf16[2048,256]{1,0:T(8,128)(2,1)} async-done(((bf16[256,256]{1,0:T(8,128)(2,1)}), bf16[2048,256]{1,0:T(8,128)(2,1)}) %all-gather.4.cloned.1.call-update) | async-done | bytes 1048592 | tf_op jit(solution)/shard_map/all_gather | solution.py:45
  54.1 6.2 %fusion.20 = f32[2048,256]{1,0:T(8,128)S(1)} fusion(bf16[2048,2048]{1,0:T(8,128)(2,1)} %param.12, bf16[2048,256]{1,0:T(8,128)(2,1)} %all-gather.4.cloned.1.call-done), kind=kOutput, calls=%fused_computation.38 | convolution fusion | flops 2147483648 | bytes 11534336 | tf_op jit(solution)/shard_map/dot_general | solution.py:44
  62.9 1.9 pad_maximum_fusion
  64.9 73.4 %reduce-scatter.4.cloned.1.call-done = f32[32,3072]{1,0:T(8,128)} async-done(((f32[256,3072]{1,0:T(8,128)}), f32[32,3072]{1,0:T(8,128)}) %reduce-scatter.4.cloned.1.call-update) | async-done | bytes 393232 | tf_op jit(solution)/shard_map/reduce_scatter | solution.py:78
  138.3 1.6 slice.8
  139.9 1.7 slice.9
  141.7 18.4 %reduce-scatter.6.cloned.1.call-done = f32[32,256]{1,0:T(8,128)} async-done(((f32[32,1024]{1,0:T(8,128)}), f32[32,256]{1,0:T(8,128)}) %reduce-scatter.6.cloned.1.call-update) | async-done | bytes 32784 | tf_op jit(solution)/shard_map/reduce_scatter | solution.py:82
  161.5 21.6 %reduce-scatter.8.cloned.1.call-done = f32[32,512]{1,0:T(8,128)} async-done(((f32[32,2048]{1,0:T(8,128)}), f32[32,512]{1,0:T(8,128)}) %reduce-scatter.8.cloned.1.call-update) | async-done | bytes 65552 | tf_op jit(solution)/shard_map/reduce_scatter | solution.py:83
  186.0 39.3 %psum.16 = f32[]{:T(128)} all-reduce(f32[]{:T(128)S(6)} %add.45), channel_id=1, replica_groups=mesh['fs'=8,'tp'=4] {'fs','tp'}, use_global_device_ids=true, to_apply=%region_3.0 | all-reduce | flops 1 | bytes 8 | tf_op jit(solution)/shard_map/psum | solution.py:85
  226.0 1.5 add_divide_fusion
  227.6 31.2 %all_gather.17 = f32[256,512]{1,0:T(8,128)S(1)} all-gather(f32[32,512]{1,0:T(8,128)S(1)} %get-tuple-element.24), channel_id=1, replica_groups=mesh['fs'=8,'tp'=4] {'fs'}, dimensions={0}, use_global_device_ids=true | all-gather | bytes 589824 | tf_op jit(solution)/shard_map/all_gather | solution.py:97
  260.8 1.5 collective-permute-start
  262.3 2.4 collective-permute-done
  264.8 4.2 %collective-permute-done.1 = f32[64,256]{1,0:T(8,128)S(1)} collective-permute-done((f32[64,256]{1,0:T(8,128)S(1)}, f32[64,256]{1,0:T(8,128)S(1)}, u32[]{:S(2)}, u32[]{:S(2)}) %collective-permute-start.1) | collective-permute-done | bytes 65568 | tf_op jit(solution)/shard_map/ppermute | solution.py:24
  269.1 1.7 collective-permute-start.2
  270.9 6.5 %collective-permute-done.2 = f32[128,256]{1,0:T(8,128)S(1)} collective-permute-done((f32[128,256]{1,0:T(8,128)S(1)}, f32[128,256]{1,0:T(8,128)S(1)}, u32[]{:S(2)}, u32[]{:S(2)}) %collective-permute-start.2) | collective-permute-done | bytes 131104 | tf_op jit(solution)/shard_map/ppermute | solution.py:24
  281.8 19.3 %all-gather.8.cloned.1.call-done = bf16[1024,512]{0,1:T(8,128)(2,1)} async-done(((bf16[128,512]{0,1:T(8,128)(2,1)}), bf16[1024,512]{0,1:T(8,128)(2,1)}) %all-gather.8.cloned.1.call-update) | async-done | bytes 1048592 | tf_op jit(solution)/shard_map/all_gather | solution.py:104
  301.2 2.3 copy.29
  303.4 38.6 %all-gather.6.cloned.1.call-done = bf16[2048,256]{0,1:T(8,128)(2,1)} async-done(((bf16[256,256]{0,1:T(8,128)(2,1)}), bf16[2048,256]{0,1:T(8,128)(2,1)}) %all-gather.6.cloned.1.call-update) | async-done | bytes 1048592 | tf_op jit(solution)/shard_map/all_gather | solution.py:103
  342.1 2.3 copy.28
  (52 shorter events, 13.2 us)
Async XLA Ops:
  7.2 46.9 %all-gather.4.cloned.1.call-start = ((), (), s32[]{:S(2)}) async-start(), calls=%async_computation.3 | async-start | bytes 1179648 | tf_op jit(solution)/shard_map/all_gather | solution.py:45
  7.9 130.4 %reduce-scatter.4.cloned.1.call-start = ((), (), s32[]{:S(2)}) async-start(), calls=%async_computation.4 | async-start | bytes 3538944 | tf_op jit(solution)/shard_map/reduce_scatter | solution.py:78
  8.0 37.1 %copy-start = (bf16[2048,2048]{1,0:T(8,128)(2,1)S(1)}, bf16[2048,2048]{1,0:T(8,128)(2,1)}, u32[]{:S(2)}) copy-start(bf16[2048,2048]{1,0:T(8,128)(2,1)} %param.15) | copy-start | bytes 25165828
  54.1 6.3 %copy-start.10 = (bf16[2048,1024]{1,0:T(8,128)(2,1)S(1)}, bf16[2048,1024]{1,0:T(8,128)(2,1)}, u32[]{:S(2)}) copy-start(bf16[2048,1024]{1,0:T(8,128)(2,1)} %param.13) | copy-start | bytes 12582916
  64.8 121.1 %copy-start.3 = (f32[128,512]{1,0:T(8,128)S(1)}, f32[128,512]{1,0:T(8,128)}, u32[]{:S(2)}) copy-start(f32[128,512]{1,0:T(8,128)} %param.19) | copy-start | bytes 786436
  64.8 161.2 %copy-start.6 = (f32[32,512]{1,0:T(8,128)S(1)}, f32[32,512]{1,0:T(8,128)}, u32[]{:S(2)}) copy-start(f32[32,512]{1,0:T(8,128)} %param.23) | copy-start | bytes 196612
  64.8 161.2 %copy-start.7 = (f32[32,512]{1,0:T(8,128)S(1)}, f32[32,512]{1,0:T(8,128)}, u32[]{:S(2)}) copy-start(f32[32,512]{1,0:T(8,128)} %param.22) | copy-start | bytes 196612
  64.8 194.0 %copy-start.2 = (bf16[128,256]{1,0:T(8,128)(2,1)S(1)}, bf16[128,256]{1,0:T(8,128)(2,1)}, u32[]{:S(2)}) copy-start(bf16[128,256]{1,0:T(8,128)(2,1)} %param.17) | copy-start | bytes 196612
  64.8 195.3 %copy-start.8 = (f32[32,256]{1,0:T(8,128)S(1)}, f32[32,256]{1,0:T(8,128)}, u32[]{:S(2)}) copy-start(f32[32,256]{1,0:T(8,128)} %param.21) | copy-start | bytes 98308
  64.8 195.3 %copy-start.9 = (f32[32,256]{1,0:T(8,128)S(1)}, f32[32,256]{1,0:T(8,128)}, u32[]{:S(2)}) copy-start(f32[32,256]{1,0:T(8,128)} %param.20) | copy-start | bytes 98308
  64.9 205.9 %copy-start.4 = (f32[256,256]{1,0:T(8,128)S(1)}, f32[256,256]{1,0:T(8,128)}, u32[]{:S(2)}) copy-start(f32[256,256]{1,0:T(8,128)} %param.18) | copy-start | bytes 786436
  64.9 212.5 %copy-start.1 = (bf16[256,256]{1,0:T(8,128)(2,1)S(1)}, bf16[256,256]{1,0:T(8,128)(2,1)}, u32[]{:S(2)}) copy-start(bf16[256,256]{1,0:T(8,128)(2,1)} %param.16) | copy-start | bytes 393220
  64.9 95.2 %reduce-scatter.6.cloned.1.call-start = ((), (), s32[]{:S(2)}) async-start(), calls=%async_computation.5 | async-start | bytes 163840 | tf_op jit(solution)/shard_map/reduce_scatter | solution.py:82
  139.9 43.2 %reduce-scatter.8.cloned.1.call-start = ((), (), s32[]{:S(2)}) async-start(), calls=%async_computation.6 | async-start | bytes 327680 | tf_op jit(solution)/shard_map/reduce_scatter | solution.py:83
  141.6 159.5 %all-gather.8.cloned.1.call-start = ((), (), s32[]{:S(2)}) async-start(), calls=%async_computation.8 | async-start | bytes 1179648 | tf_op jit(solution)/shard_map/all_gather | solution.py:104
  160.1 100.1 %copy-start.5 = (f32[32,256]{1,0:T(8,128)S(1)}, f32[32,256]{1,0:T(8,128)}, u32[]{:S(2)}) copy-start(f32[32,256]{1,0:T(8,128)} %reduce-scatter.6.cloned.1.call-done) | copy-start | bytes 98308
  260.1 82.0 %all-gather.6.cloned.1.call-start = ((), (), s32[]{:S(2)}) async-start(), calls=%async_computation.7 | async-start | bytes 1179648 | tf_op jit(solution)/shard_map/all_gather | solution.py:103
  260.8 3.9 %collective-permute-start = (f32[32,256]{1,0:T(8,128)S(1)}, f32[32,256]{1,0:T(8,128)S(1)}, u32[]{:S(2)}, u32[]{:S(2)}) collective-permute-start(f32[32,256]{1,0:T(8,128)S(1)} %get-tuple-element.27), channel_id=1, source_target_pairs={{0,4},{4,0},{8,12},{12,8},{16,20},{20,16},{24,28},{28,24},{1,5},{5... | collective-permute-start | bytes 98312 | tf_op jit(solution)/shard_map/ppermute | solution.py:24
  264.7 4.3 %collective-permute-start.1 = (f32[64,256]{1,0:T(8,128)S(1)}, f32[64,256]{1,0:T(8,128)S(1)}, u32[]{:S(2)}, u32[]{:S(2)}) collective-permute-start(f32[64,256]{1,0:T(8,128)S(1)} %maximum_select_fusion.3), channel_id=1, source_target_pairs={{0,8},{4,12},{8,0},{12,4},{16,24},{20,28},{24,16},{28,20},{1,9},{5... | collective-permute-start | bytes 196616 | tf_op jit(solution)/shard_map/ppermute | solution.py:24
  269.1 8.3 %collective-permute-start.2 = (f32[128,256]{1,0:T(8,128)S(1)}, f32[128,256]{1,0:T(8,128)S(1)}, u32[]{:S(2)}, u32[]{:S(2)}) collective-permute-start(f32[128,256]{1,0:T(8,128)S(1)} %maximum_select_fusion.2), channel_id=1, source_target_pairs={{0,16},{4,20},{8,24},{12,28},{16,0},{20,4},{24,8},{28,12},{1,17},{... | collective-permute-start | bytes 393224 | tf_op jit(solution)/shard_map/ppermute | solution.py:24
Sparse Core Ops, SparseCore 0:
  10.1 43.9 all-gather.3
  65.0 73.2 reduce-scatter.3
  141.3 18.7 reduce-scatter.5
  163.0 20.0 reduce-scatter.7
  260.2 40.9 all-gather.7
  303.6 38.3 all-gather.5
